TPU v7x, 512 devices: a whole 4x4x16 slice. The times are simulated.
512 devices in a mesh: ra: 16 (over y, x), cb: 32 (over z, core).
Axes of the slice: x: 4, y: 4, z: 16, core: 2. Of those that a mesh axis runs over, the one named last changes fastest.
Arguments:
- tokens: bfloat16 [256, 4096], P(None, 'ra'), may hold values from -20 to 20, as said below
- norm_gain: float32 [2, 4096], P(None, 'ra'), may hold values from 0.1 to 1.9
- gate_weight: bfloat16 [2, 4096, 11008], P(None, 'ra', 'cb'), may hold values from -0.09375 to 0.09375
- value_weight: bfloat16 [2, 4096, 11008], P(None, 'ra', 'cb'), may hold values from -0.09375 to 0.09375
- gate_taps: float32 [2, 3, 11008], P(None, None, 'cb'), may hold values from -3.5 to 3.5
- value_taps: float32 [2, 3, 11008], P(None, None, 'cb'), may hold values from -3.5 to 3.5
- down_weight: bfloat16 [2, 11008, 4096], P(None, 'cb', 'ra'), may hold values from -0.0546875 to 0.0546875
Outputs:
- mixed: bfloat16 [256, 4096], P(None, 'ra')
Inputs may be any that keep to these rules, and one draw needn't show every extreme that they name: tokens have features drawn around zero with a scale that varies by blocks of features between about 0.3 and 3.3.
All inputs are finite; a program needn't handle non-finite values.
Results may differ from a plain program's by a relative error of at most 0.0075.
Values may be sent and summed in bfloat16 or wider, within the bound.
A program may use at most 128 MiB of HBM per device.

v0:
```python
import jax
import jax.numpy as jnp
from jax import lax
from jax.sharding import Mesh
from jax.sharding import PartitionSpec as P

D = 4096
RA = ("ra_0", "ra_1")
epsilon = 1e-06


def laid_out(parts, dim):
    shape = list(parts.shape[1:])
    shape[dim] *= parts.shape[0]
    return jnp.moveaxis(parts, 0, dim).reshape(shape)


def copy_for_each(array, axis):
    copies = jnp.broadcast_to(array, (lax.axis_size(axis), *array.shape))
    return lax.all_to_all(copies, axis, split_axis=0, concat_axis=0, tiled=True)


def gathered_copies(array, axis, dim):
    return laid_out(copy_for_each(array, axis), dim)


def shifted(block, axis, distance):
    devices = range(lax.axis_size(axis))
    route = [(i - distance, i) for i in devices if i - distance in devices]
    return lax.ppermute(block, axis, route)


def over_pieces(array, axis):
    return lax.all_gather(array, axis).sum(0)


def split_up(array, dim, peers):
    before, after = (array.shape[:dim], array.shape[dim + 1 :])
    return jnp.moveaxis(array.reshape(*before, peers, -1, *after), dim, 0)


def moved_by_axis(parts, axes, order):
    shape = [lax.axis_size(a) for a in axes]
    parts = parts.reshape(*shape, *parts.shape[1:])
    for k in order:
        parts = lax.all_to_all(parts, axes[k], split_axis=k, concat_axis=k, tiled=True)
    return parts.reshape(-1, *parts.shape[len(axes) :])


def stepwise_exchange(array, axes, order, split_dim, concat_dim):
    parts = split_up(array, split_dim, lax.axis_size(axes))
    return laid_out(moved_by_axis(parts, axes, order), concat_dim)


def conv_after(signal, earlier, kernel_taps):
    length = signal.shape[0]
    width = kernel_taps.shape[0]
    padded = jnp.concatenate([earlier, signal], axis=0)
    result = jnp.zeros(signal.shape, jnp.float32)
    for offset in range(width):
        result = result + kernel_taps[offset] * padded[offset : offset + length]
    return result


def body(tokens, norm_gain, gate_weight, value_weight, gate_taps, value_taps, down_weight):
    stream = lax.all_to_all(tokens, RA, split_axis=0, concat_axis=1, tiled=True)
    gate_whole, value_whole, down_whole = (
        lax.all_gather(gate_weight, RA, axis=1, tiled=True),
        lax.all_gather(value_weight, RA, axis=1, tiled=True),
        lax.all_gather(down_weight, RA, axis=2, tiled=True),
    )
    gain_whole = gathered_copies(norm_gain, RA, 1)
    reach = gate_taps.shape[1] - 1
    for layer_index in range(gate_weight.shape[0]):
        current = stream.astype(jnp.float32)
        inverse_rms = lax.rsqrt(jnp.sum(current * current, axis=1, keepdims=True) / D + epsilon)
        scaled = (current * gain_whole[layer_index]).astype(jnp.bfloat16)
        gate_lin = (
            jnp.dot(scaled, gate_whole[layer_index], preferred_element_type=jnp.float32)
            * inverse_rms
        )
        value_lin = (
            jnp.dot(scaled, value_whole[layer_index], preferred_element_type=jnp.float32)
            * inverse_rms
        )
        tails = jnp.stack(
            [gate_lin[gate_lin.shape[0] - reach :], value_lin[value_lin.shape[0] - reach :]]
        )
        earlier = shifted(tails, RA, 1)
        gate_conv = conv_after(gate_lin, earlier[0], gate_taps[layer_index])
        value_conv = conv_after(value_lin, earlier[1], value_taps[layer_index])
        hidden = (jax.nn.silu(gate_conv) * value_conv).astype(jnp.bfloat16)
        partial_branch = jnp.dot(
            hidden, down_whole[layer_index], preferred_element_type=jnp.float32
        )
        branch = over_pieces(partial_branch, "cb")
        stream = (0.5 * current + branch).astype(jnp.bfloat16)
    return stepwise_exchange(stream, RA, (0, 1), 1, 0)


def solution(mesh):
    finer = Mesh(mesh.devices.reshape(4, 4, mesh.shape["cb"]), ("ra_0", "ra_1", "cb"))
    placed = (
        P(None, RA),
        P(None, RA),
        P(None, RA, "cb"),
        P(None, RA, "cb"),
        P(None, None, "cb"),
        P(None, None, "cb"),
        P(None, "cb", RA),
    )
    return jax.shard_map(body, mesh=finer, in_specs=placed, out_specs=P(None, RA), check_vma=False)
```

profile of v0, /device:TPU:32, one launch (start us, length us, event | category | flops | bytes accessed | tf_op | source)
XLA Modules:
  0.0 463.0 jit_solution(13251371283180898121)
XLA Ops:
  6.5 0.0 copy-start
  6.5 0.0 copy-start.1
  6.5 0.0 all-gather.8.cloned.1.call-start
  6.5 0.7 all-gather.8.cloned.1.call-update
  7.3 0.0 all-gather.10.cloned.1.call-start
  7.3 0.7 all-gather.10.cloned.1.call-update
  8.0 0.0 all-gather.12.cloned.1.call-start
  8.1 0.7 all-gather.12.cloned.1.call-update
  8.7 0.7 broadcast_in_dim.2
  9.4 14.4 %all_to_all.28 = f32[16,2,256]{2,1,0:T(2,128)S(1)} all-to-all(f32[16,2,256]{2,1,0:T(2,128)S(1)} %broadcast_in_dim.2), channel_id=1, replica_groups=mesh['ra_0'=4,'ra_1'=4,'cb'=32] {'ra_0','ra_1'}, dimensions={0} | all-to-all | bytes 65536 | tf_op jit(solution)/shard_map/all_to_all | solution.py:20
  23.9 3.5 all-to-all-start
  27.4 0.0 all-gather.14.cloned.1.call-start
  27.5 7.9 %all-to-all-done = bf16[16,16,256]{2,1,0:T(8,128)(2,1)S(1)} async-done(((bf16[16,16,256]{2,1,0:T(8,128)(2,1)}), bf16[16,16,256]{2,1,0:T(8,128)(2,1)S(1)}, u32[]{:S(2)}, u32[]{:S(2)}) %all-to-all-start) | async-done | bytes 131104 | tf_op jit(solution)/shard_map/all_to_all | solution.py:66
  35.4 0.2 fusion.10
  35.5 57.9 %all-gather.8.cloned.1.call-done = bf16[2,4096,344]{1,2,0:T(8,128)(2,1)} async-done(((bf16[2,256,344]{1,2,0:T(8,128)(2,1)}), bf16[2,4096,344]{1,2,0:T(8,128)(2,1)}) %all-gather.8.cloned.1.call-update) | async-done | bytes 5636112 | tf_op jit(solution)/shard_map/all_gather | solution.py:68
  93.5 2.6 fusion.6
  96.1 78.8 %all-gather.10.cloned.1.call-done = bf16[2,4096,344]{1,2,0:T(8,128)(2,1)} async-done(((bf16[2,256,344]{1,2,0:T(8,128)(2,1)}), bf16[2,4096,344]{1,2,0:T(8,128)(2,1)}) %all-gather.10.cloned.1.call-update) | async-done | bytes 5636112 | tf_op jit(solution)/shard_map/all_gather | solution.py:69
  174.9 2.6 fusion.7
  177.6 3.1 collective-permute-start
  180.7 0.0 copy-done
  180.7 0.0 copy-done.1
  180.7 0.1 slice_reduce_fusion.2
  180.8 1.2 collective-permute-done
  182.0 74.4 %all-gather.12.cloned.1.call-done = bf16[2,344,4096]{2,1,0:T(8,128)(2,1)} async-done(((bf16[2,344,256]{2,1,0:T(8,128)(2,1)}), bf16[2,344,4096]{2,1,0:T(8,128)(2,1)}) %all-gather.12.cloned.1.call-update) | async-done | bytes 5636112 | tf_op jit(solution)/shard_map/all_gather | solution.py:70
  256.4 3.1 fusion.3
  259.5 0.0 all-gather.14.cloned.1.call-update
  259.6 0.0 all-gather.16.cloned.1.call-start
  259.6 78.3 %all-gather.14.cloned.1.call-done = f32[512,4096]{1,0:T(8,128)} async-done(((f32[16,4096]{1,0:T(8,128)}), f32[512,4096]{1,0:T(8,128)}) %all-gather.14.cloned.1.call-update) | async-done | bytes 8388624 | tf_op jit(solution)/shard_map/all_gather | solution.py:34
  338.0 3.8 reduce_sum.41
  341.7 0.1 copy.24
  341.8 0.3 fusion.16
  342.2 2.6 fusion.8
  344.9 2.6 fusion.9
  347.5 3.3 collective-permute-start.1
  350.8 1.3 collective-permute-done.1
  352.1 3.1 fusion
  355.2 0.0 all-gather.16.cloned.1.call-update
  355.2 76.4 %all-gather.16.cloned.1.call-done = f32[512,4096]{1,0:T(8,128)} async-done(((f32[16,4096]{1,0:T(8,128)}), f32[512,4096]{1,0:T(8,128)}) %all-gather.16.cloned.1.call-update) | async-done | bytes 8388624 | tf_op jit(solution)/shard_map/all_gather | solution.py:34
  431.7 3.8 reduce_sum.44
  435.5 0.1 copy.26
  435.7 9.9 %all_to_all.29 = bf16[4,4,16,256]{3,1,2,0:T(4,128)(2,1)S(1)} all-to-all(bf16[4,4,16,256]{3,1,2,0:T(4,128)(2,1)S(1)} %copy.18), channel_id=1, replica_groups=mesh['ra_0'=4,'ra_1'=4,'cb'=32] {'ra_0'}, dimensions={0} | all-to-all | bytes 262144 | tf_op jit(solution)/shard_map/all_to_all | solution.py:46
  445.6 0.1 copy.19
  445.7 10.0 %all_to_all.30 = bf16[4,4,16,256]{3,0,2,1:T(4,128)(2,1)S(1)} all-to-all(bf16[4,4,16,256]{3,0,2,1:T(4,128)(2,1)S(1)} %copy.19), channel_id=1, replica_groups=mesh['ra_0'=4,'ra_1'=4,'cb'=32] {'ra_1'}, dimensions={1} | all-to-all | bytes 262144 | tf_op jit(solution)/shard_map/all_to_all | solution.py:46
  455.8 0.7 copy.20
  (19 shorter events, 0.3 us)
Async XLA Ops:
  6.5 174.2 %copy-start = (f32[2,3,344]{2,0,1:T(2,128)S(1)}, f32[2,3,344]{2,0,1:T(2,128)}, u32[]{:S(2)}) copy-start(f32[2,3,344]{2,0,1:T(2,128)} %param.12) | copy-start | bytes 24772
  6.5 174.2 %copy-start.1 = (f32[2,3,344]{2,0,1:T(2,128)S(1)}, f32[2,3,344]{2,0,1:T(2,128)}, u32[]{:S(2)}) copy-start(f32[2,3,344]{2,0,1:T(2,128)} %param.11) | copy-start | bytes 24772
  6.5 86.9 %all-gather.8.cloned.1.call-start = ((), (), s32[]{:S(2)}) async-start(), calls=%async_computation.4 | async-start | bytes 5988352 | tf_op jit(solution)/shard_map/all_gather | solution.py:68
  7.3 167.7 %all-gather.10.cloned.1.call-start = ((), (), s32[]{:S(2)}) async-start(), calls=%async_computation.5 | async-start | bytes 5988352 | tf_op jit(solution)/shard_map/all_gather | solution.py:69
  8.0 248.4 %all-gather.12.cloned.1.call-start = ((), (), s32[]{:S(2)}) async-start(), calls=%async_computation.6 | async-start | bytes 5988352 | tf_op jit(solution)/shard_map/all_gather | solution.py:70
  23.9 11.5 %all-to-all-start = ((bf16[16,16,256]{2,1,0:T(8,128)(2,1)}), bf16[16,16,256]{2,1,0:T(8,128)(2,1)S(1)}, u32[]{:S(2)}, u32[]{:S(2)}) async-start(bf16[16,16,256]{2,1,0:T(8,128)(2,1)} %bitcast.87), calls=%async_computation | async-start | bytes 262144 | tf_op jit(solution)/shard_map/all_to_all | solution.py:66
  27.4 310.6 %all-gather.14.cloned.1.call-start = ((), (), s32[]{:S(2)}) async-start(), calls=%async_computation.7 | async-start | bytes 8650752 | tf_op jit(solution)/shard_map/all_gather | solution.py:34
  177.6 4.4 collective-permute-start
  259.6 172.1 %all-gather.16.cloned.1.call-start = ((), (), s32[]{:S(2)}) async-start(), calls=%async_computation.8 | async-start | bytes 8650752 | tf_op jit(solution)/shard_map/all_gather | solution.py:34
  347.5 4.6 collective-permute-start.1
Sparse Core Ops, SparseCore 0:
  10.3 83.0 all-gather.7
  96.4 78.4 all-gather.9
  177.9 78.4 all-gather.11
  259.7 78.2 all-gather.13
  355.4 76.2 all-gather.15
where the time goes:
time: 464 us; the launch traced here: 463 us
  waiting for transfers between devices  378 us (81%)
  blocking collectives  34.4 us (7%)
  matrix products  16.7 us (4%)
  between operations  13.4 us (3%)
  starting transfers between devices  10 us (2%)
  other arithmetic  8.1 us (2%)
    all_gather x2, waiting for transfers between devices, over_pieces(): return lax.all_gather(array, axis).sum(0)  155 us
    all_gather x1, waiting for transfers between devices, body(): lax.all_gather(value_weight, RA, axis=1, tiled=True)  78.8 us
    all_gather x1, waiting for transfers between devices, body(): lax.all_gather(down_weight, RA, axis=2, tiled=True)  74.4 us
    all_gather x1, waiting for transfers between devices, body(): lax.all_gather(gate_weight, RA, axis=1, tiled=True)  57.9 us
    all_to_all x2, blocking collectives, moved_by_axis(): lax.all_to_all(parts, axes[k], split_axis=k, concat_axis=k, tiled=True)  20 us
    all_to_all x1, blocking collectives, copy_for_each(): return lax.all_to_all(copies, axis, split_axis=0, concat_axis=0, tiled=True)  14.4 us
  transfers between devices with their start and end apart: 8, of which 8 were waited for; matrix products, arithmetic and copies ran while one was open for 1% of the time, Pallas kernels for 0%

commit v1 on v0

--- a/solution.py
+++ b/solution.py
@@ -67,7 +67,9 @@
     gate_whole, value_whole, down_whole = (
         lax.all_gather(gate_weight, RA, axis=1, tiled=True),
         lax.all_gather(value_weight, RA, axis=1, tiled=True),
-        lax.all_gather(down_weight, RA, axis=2, tiled=True),
+        jnp.concatenate(
+            lax.all_to_all(jnp.stack([down_weight] * lax.axis_size(RA)), RA, 0, 0), axis=2
+        ),
     )
     gain_whole = gathered_copies(norm_gain, RA, 1)
     reach = gate_taps.shape[1] - 1

time: 464 us -> 443 us (0.955)
  waiting for transfers between devices: 378 us -> 341 us
  blocking collectives: 34.4 us -> 45.9 us
  local copies, waits for them, and re-layouts: 1.91 us -> 9.41 us
    all_gather x1 -> x0, waiting for transfers between devices: 74.4 us -> none  [body(): lax.all_gather(down_weight, RA, axis=2, tiled=True)]
    all_gather x1, waiting for transfers between devices: 57.9 us -> 99.1 us  [body(): lax.all_gather(gate_weight, RA, axis=1, tiled=True)]
    all_to_all x0 -> x1, blocking collectives: none -> 11.5 us  [body(): stream = lax.all_to_all(tokens, RA, split_axis=0, concat_axis=1, tiled=True)]
    all_to_all x1, waiting for transfers between devices: 7.86 us -> 0.01 us  [body(): lax.all_to_all(jnp.stack([down_weight] * lax.axis_size(RA)), RA, 0, 0)]
    all_gather x1, waiting for transfers between devices: 78.8 us -> 83.9 us  [body(): lax.all_gather(value_weight, RA, axis=1, tiled=True)]
  transfers between devices with their start and end apart: 8 -> 7, of which waited for: 8 -> 5; matrix products, arithmetic and copies ran while one was open for 1% -> 3% of each run, Pallas kernels for 0% -> 0%
where the time goes in v1:
time: 443 us
  waiting for transfers between devices  341 us (77%)
  blocking collectives  45.9 us (10%)
  between operations  13.4 us (3%)
  matrix products  13.1 us (3%)
  starting transfers between devices  11.2 us (3%)
  local copies, waits for them, and re-layouts  9.41 us (2%)
  other arithmetic  8.1 us (2%)
    all_gather x2, waiting for transfers between devices, over_pieces(): return lax.all_gather(array, axis).sum(0)  156 us
    all_gather x1, waiting for transfers between devices, body(): lax.all_gather(gate_weight, RA, axis=1, tiled=True)  99.1 us
    all_gather x1, waiting for transfers between devices, body(): lax.all_gather(value_weight, RA, axis=1, tiled=True)  83.9 us
    all_to_all x2, blocking collectives, moved_by_axis(): lax.all_to_all(parts, axes[k], split_axis=k, concat_axis=k, tiled=True)  20 us
    all_to_all x1, blocking collectives, copy_for_each(): return lax.all_to_all(copies, axis, split_axis=0, concat_axis=0, tiled=True)  14.4 us
    all_to_all x1, blocking collectives, body(): stream = lax.all_to_all(tokens, RA, split_axis=0, concat_axis=1, tiled=True)  11.5 us
  transfers between devices with their start and end apart: 7, of which 5 were waited for; matrix products, arithmetic and copies ran while one was open for 3% of the time, Pallas kernels for 0%

profile of v1, /device:TPU:32, one launch (start us, length us, event | category | flops | bytes accessed | tf_op | source)
XLA Modules:
  0.0 442.5 jit_solution(12750947449805139925)
XLA Ops:
  6.5 0.0 all-gather.7.cloned.1.call-start
  6.5 0.7 all-gather.7.cloned.1.call-update
  7.3 0.0 all-gather.9.cloned.1.call-start
  7.3 0.7 all-gather.9.cloned.1.call-update
  8.0 0.7 broadcast_in_dim.2
  8.7 14.4 %all_to_all.33 = f32[16,2,256]{2,1,0:T(2,128)S(1)} all-to-all(f32[16,2,256]{2,1,0:T(2,128)S(1)} %broadcast_in_dim.2), channel_id=1, replica_groups=mesh['ra_0'=4,'ra_1'=4,'cb'=32] {'ra_0','ra_1'}, dimensions={0} | all-to-all | bytes 65536 | tf_op jit(solution)/shard_map/all_to_all | solution.py:20
  23.1 11.5 %all_to_all.34 = bf16[16,16,256]{2,1,0:T(8,128)(2,1)S(1)} all-to-all(bf16[16,16,256]{2,1,0:T(8,128)(2,1)} %bitcast.96), channel_id=1, replica_groups=mesh['ra_0'=4,'ra_1'=4,'cb'=32] {'ra_0','ra_1'}, dimensions={0} | all-to-all | bytes 262144 | tf_op jit(solution)/shard_map/all_to_all | solution.py:66
  34.6 3.8 stack.17
  38.4 0.0 copy-start
  38.4 0.0 copy-start.1
  38.4 4.7 %all-to-all-start.2 = ((bf16[16,2,344,256]{3,2,1,0:T(8,128)(2,1)}), bf16[16,2,344,256]{3,2,1,0:T(8,128)(2,1)}, u32[]{:S(2)}, u32[]{:S(2)}) async-start(bf16[16,2,344,256]{3,2,1,0:T(8,128)(2,1)} %stack.17), calls=%async_computation.2 | async-start | bytes 11272192 | tf_op jit(solution)/shard_map/all_to_all | solution.py:71
  43.1 0.0 all-gather.11.cloned.1.call-start
  43.2 0.0 copy-done
  43.2 0.0 copy-done.1
  43.2 0.1 slice_reduce_fusion.2
  43.3 0.2 fusion.8
  43.5 99.1 %all-gather.7.cloned.1.call-done = bf16[2,4096,344]{1,2,0:T(8,128)(2,1)} async-done(((bf16[2,256,344]{1,2,0:T(8,128)(2,1)}), bf16[2,4096,344]{1,2,0:T(8,128)(2,1)}) %all-gather.7.cloned.1.call-update) | async-done | bytes 5636112 | tf_op jit(solution)/shard_map/all_gather | solution.py:68
  142.6 2.6 fusion.4
  145.2 83.9 %all-gather.9.cloned.1.call-done = bf16[2,4096,344]{1,2,0:T(8,128)(2,1)} async-done(((bf16[2,256,344]{1,2,0:T(8,128)(2,1)}), bf16[2,4096,344]{1,2,0:T(8,128)(2,1)}) %all-gather.9.cloned.1.call-update) | async-done | bytes 5636112 | tf_op jit(solution)/shard_map/all_gather | solution.py:69
  229.2 2.6 fusion.5
  231.9 3.1 collective-permute-start
  234.9 0.0 all-to-all-done.2
  235.0 3.0 fusion.64
  238.0 0.3 copy.28
  238.3 0.0 collective-permute-done
  238.4 1.3 fusion.41
  239.7 0.0 all-gather.11.cloned.1.call-update
  239.7 0.0 all-gather.13.cloned.1.call-start
  239.8 79.6 %all-gather.11.cloned.1.call-done = f32[512,4096]{1,0:T(8,128)} async-done(((f32[16,4096]{1,0:T(8,128)}), f32[512,4096]{1,0:T(8,128)}) %all-gather.11.cloned.1.call-update) | async-done | bytes 8388624 | tf_op jit(solution)/shard_map/all_gather | solution.py:34
  319.3 3.8 reduce_sum.41
  323.1 0.1 copy.29
  323.2 0.3 fusion.14
  323.6 2.6 fusion.6
  326.2 2.6 fusion.7
  328.9 3.3 collective-permute-start.1
  332.2 0.3 copy.31
  332.5 1.0 collective-permute-done.1
  333.5 1.3 fusion.43
  334.8 0.0 all-gather.13.cloned.1.call-update
  334.8 76.4 %all-gather.13.cloned.1.call-done = f32[512,4096]{1,0:T(8,128)} async-done(((f32[16,4096]{1,0:T(8,128)}), f32[512,4096]{1,0:T(8,128)}) %all-gather.13.cloned.1.call-update) | async-done | bytes 8388624 | tf_op jit(solution)/shard_map/all_gather | solution.py:34
  411.2 3.8 reduce_sum.44
  415.0 0.1 copy.32
  415.3 9.9 %all_to_all.35 = bf16[4,4,16,256]{3,1,2,0:T(4,128)(2,1)S(1)} all-to-all(bf16[4,4,16,256]{3,1,2,0:T(4,128)(2,1)S(1)} %copy.22), channel_id=1, replica_groups=mesh['ra_0'=4,'ra_1'=4,'cb'=32] {'ra_0'}, dimensions={0} | all-to-all | bytes 262144 | tf_op jit(solution)/shard_map/all_to_all | solution.py:46
  425.2 0.1 copy.23
  425.3 10.0 %all_to_all.36 = bf16[4,4,16,256]{3,0,2,1:T(4,128)(2,1)S(1)} all-to-all(bf16[4,4,16,256]{3,0,2,1:T(4,128)(2,1)S(1)} %copy.23), channel_id=1, replica_groups=mesh['ra_0'=4,'ra_1'=4,'cb'=32] {'ra_1'}, dimensions={1} | all-to-all | bytes 262144 | tf_op jit(solution)/shard_map/all_to_all | solution.py:46
  435.3 0.7 copy.24
  (19 shorter events, 0.3 us)
Async XLA Ops:
  6.5 136.0 %all-gather.7.cloned.1.call-start = ((), (), s32[]{:S(2)}) async-start(), calls=%async_computation.5 | async-start | bytes 5988352 | tf_op jit(solution)/shard_map/all_gather | solution.py:68
  7.3 221.9 %all-gather.9.cloned.1.call-start = ((), (), s32[]{:S(2)}) async-start(), calls=%async_computation.6 | async-start | bytes 5988352 | tf_op jit(solution)/shard_map/all_gather | solution.py:69
  38.4 4.8 %copy-start = (f32[2,3,344]{2,0,1:T(2,128)S(1)}, f32[2,3,344]{2,0,1:T(2,128)}, u32[]{:S(2)}) copy-start(f32[2,3,344]{2,0,1:T(2,128)} %param.12) | copy-start | bytes 24772
  38.4 4.8 %copy-start.1 = (f32[2,3,344]{2,0,1:T(2,128)S(1)}, f32[2,3,344]{2,0,1:T(2,128)}, u32[]{:S(2)}) copy-start(f32[2,3,344]{2,0,1:T(2,128)} %param.11) | copy-start | bytes 24772
  38.4 196.6 %all-to-all-start.2 = ((bf16[16,2,344,256]{3,2,1,0:T(8,128)(2,1)}), bf16[16,2,344,256]{3,2,1,0:T(8,128)(2,1)}, u32[]{:S(2)}, u32[]{:S(2)}) async-start(bf16[16,2,344,256]{3,2,1,0:T(8,128)(2,1)} %stack.17), calls=%async_computation.2 | async-start | bytes 11272192 | tf_op jit(solution)/shard_map/all_to_all | solution.py:71
  43.1 276.2 %all-gather.11.cloned.1.call-start = ((), (), s32[]{:S(2)}) async-start(), calls=%async_computation.7 | async-start | bytes 8650752 | tf_op jit(solution)/shard_map/all_gather | solution.py:34
  231.9 6.5 %collective-permute-start = (f32[2,2,344]{2,1,0:T(2,128)S(1)}, f32[2,2,344]{2,1,0:T(2,128)S(1)}, u32[]{:S(2)}, u32[]{:S(2)}) collective-permute-start(f32[2,2,344]{2,1,0:T(2,128)S(1)} %pad_maximum_fusion.4), channel_id=1, source_target_pairs={{0,32},{32,64},{64,96},{96,128},{128,160},{160,192},{192,224},{224... | collective-permute-start | bytes 16520 | tf_op jit(solution)/shard_map/ppermute | solution.py:30
  239.7 171.6 %all-gather.13.cloned.1.call-start = ((), (), s32[]{:S(2)}) async-start(), calls=%async_computation.8 | async-start | bytes 8650752 | tf_op jit(solution)/shard_map/all_gather | solution.py:34
  328.9 4.6 %collective-permute-start.1 = (f32[2,2,344]{2,1,0:T(2,128)S(1)}, f32[2,2,344]{2,1,0:T(2,128)S(1)}, u32[]{:S(2)}, u32[]{:S(2)}) collective-permute-start(f32[2,2,344]{2,1,0:T(2,128)S(1)} %pad_maximum_fusion.5), channel_id=1, source_target_pairs={{0,32},{32,64},{64,96},{96,128},{128,160},{160,192},{192,224},{224... | collective-permute-start | bytes 16520 | tf_op jit(solution)/shard_map/ppermute | solution.py:30
Sparse Core Ops, SparseCore 0:
  10.3 132.2 all-gather.6
  145.6 83.5 all-gather.8
  239.8 79.4 all-gather.10
  334.9 76.2 all-gather.12
